TPU v7x, 32 devices: a whole 2x2x4 slice. The times are simulated.
32 devices in a mesh: sp: 8 (over z, y), tp: 4 (over x, core).
Axes of the slice: x: 2, y: 2, z: 4, core: 2. Of those that a mesh axis runs over, the one named last changes fastest.
Arguments:
- queries: bfloat16 [6144, 2048], P('sp', 'tp'), may hold values from -11 to 11
- key_rows: bfloat16 [6144, 2048], P('sp', 'tp'), may hold values from -4.5 to 4.5
- value_rows: bfloat16 [6144, 2048], P('sp', 'tp'), may hold values from -6 to 6
- log_forget: float32 [6144, 32], P('sp', 'tp'), may hold values from -740.28 to 0, as said below
- stream_in: bfloat16 [6144, 2048], P('sp'), may hold values from -6 to 6
- out_weight: bfloat16 [2048, 2048], P('tp'), may hold values from -0.52734375 to 0.52734375
- mix_gain: float32 [2048], replicated, may hold values from 0.1 to 1.9
- mix_bias: float32 [2048], replicated, may hold values from -3 to 3
- gate_weight: bfloat16 [2048, 5632], P('sp', 'tp'), may hold values from -0.125 to 0.125
- up_weight: bfloat16 [2048, 5632], P('sp', 'tp'), may hold values from -0.125 to 0.125
- down_weight: bfloat16 [5632, 2048], P('tp', 'sp'), may hold values from -0.15917969 to 0.15917969
- ffn_gain: float32 [2048], replicated, may hold values from 0.1 to 1.9
- ffn_bias: float32 [2048], replicated, may hold values from -3 to 3
Outputs:
- layer_out: bfloat16 [6144, 2048], P(('sp', 'tp'))
Inputs may be any that keep to these rules, and one draw needn't show every extreme that they name: `log_forget`: each column never rises along the positions.
All inputs are finite; a program needn't handle non-finite values.
Results may differ from a plain program's by a relative error of at most 0.015.
Values may be sent and summed in bfloat16 or wider, within the bound.
A program may use at most 128 MiB of HBM per device.

v0:
```python
import jax
import jax.numpy as jnp
from jax import lax
from jax.sharding import PartitionSpec as P

ALPHA = 8.0**0.25
EPSILON = 1e-05


def layer_norm(matrix, norm_gain, norm_shift):
    centred = matrix - jnp.mean(matrix, axis=-1, keepdims=True)
    spread = jnp.mean(centred * centred, axis=-1, keepdims=True)
    return centred * lax.rsqrt(spread + EPSILON) * norm_gain + norm_shift


def attend(queries, key_rows, value_rows, log_forget):
    length, row_width = queries.shape
    head_count = log_forget.shape[1]
    head_dim = row_width // head_count
    score_scale = head_dim ** (-0.5)
    first_pos = lax.axis_index("sp") * length
    last_pos = first_pos + length
    query_heads = queries.reshape(length, head_count, head_dim)
    query_gates = log_forget.T
    query_pos = first_pos + jnp.arange(length, dtype=jnp.int32)
    gates_all = lax.all_gather(log_forget, "sp", axis=0, tiled=True)
    initial = (
        jnp.full((head_count, length), -1e30, jnp.float32),
        jnp.zeros((head_count, length), jnp.float32),
        jnp.zeros((length, head_count, head_dim), jnp.float32),
    )
    running = initial
    key_piece = lax.all_gather(key_rows, "sp", axis=0, tiled=True)
    value_piece = lax.all_gather(value_rows, "sp", axis=0, tiled=True)
    piece_len = key_piece.shape[0]
    shards = piece_len // length
    group_size = max(
        [
            count_try
            for count_try in range(1, shards + 1)
            if shards % count_try == 0 and count_try * length <= max(length, 512)
        ]
    )
    block_len = group_size * length
    blocks = piece_len // block_len
    key_blocks = key_piece.reshape(blocks, block_len, head_count, head_dim)
    value_blocks = value_piece.reshape(blocks, block_len, head_count, head_dim)
    gate_blocks = gates_all.reshape(blocks, block_len, head_count)
    block_starts = block_len * jnp.arange(blocks, dtype=jnp.int32)

    def one_block(running_state, packed):
        key_block, value_block, gate_block, block_start = packed

        def compute(state_in):
            highest, totals, weighted = state_in
            scores = (
                jnp.einsum(
                    "qhd,khd->hqk", query_heads, key_block, preferred_element_type=jnp.float32
                )
                * score_scale
            )
            scores = scores + query_gates[:, :, None] - gate_block.T[:, None, :]
            key_pos = block_start + jnp.arange(block_len, dtype=jnp.int32)
            allowed = (key_pos[None, :] <= query_pos[:, None])[None]
            masked = jnp.where(allowed, scores, -1e30)
            new_high = jnp.maximum(highest, jnp.max(masked, axis=2))
            weights = jnp.where(allowed, jnp.exp(masked - new_high[:, :, None]), 0.0)
            factor = jnp.exp(highest - new_high)
            totals = totals * factor + jnp.sum(weights, axis=2)
            weighted = weighted * factor.T[:, :, None] + jnp.einsum(
                "hqk,khd->qhd",
                weights.astype(jnp.bfloat16),
                value_block,
                preferred_element_type=jnp.float32,
            )
            return (new_high, totals, weighted)

        def keep_state(state_in):
            return state_in

        return (lax.cond(block_start < last_pos, compute, keep_state, running_state), None)

    running, unused = lax.scan(
        one_block, running, (key_blocks, value_blocks, gate_blocks, block_starts)
    )
    highest, totals, weighted = running
    return (weighted / totals.T[:, :, None]).reshape(length, row_width).astype(jnp.bfloat16)


def body(
    queries,
    key_rows,
    value_rows,
    log_forget,
    stream_in,
    out_weight,
    mix_gain,
    mix_bias,
    gate_weight,
    up_weight,
    down_weight,
    ffn_gain,
    ffn_bias,
):
    attended = attend(queries, key_rows, value_rows, log_forget)
    length = attended.shape[0]
    own_rows = length // lax.axis_size("tp")
    offset = lax.axis_index("tp") * own_rows
    summed = lax.psum_scatter(
        jnp.dot(attended, out_weight, preferred_element_type=jnp.float32).astype(jnp.bfloat16),
        "tp",
        scatter_dimension=0,
        tiled=True,
    )
    mix_out = lax.optimization_barrier(summed).astype(jnp.float32)
    stream_own = lax.dynamic_slice_in_dim(stream_in, offset, own_rows, 0)
    normed = layer_norm(
        ALPHA * stream_own.astype(jnp.float32) + mix_out, mix_gain, mix_bias
    ).astype(jnp.bfloat16)
    gathered = lax.all_gather(normed, "tp", axis=0, tiled=True)
    gate_part = jnp.dot(
        gathered,
        lax.all_gather(gate_weight, "sp", axis=0, tiled=True),
        preferred_element_type=jnp.float32,
    )
    up_part = jnp.dot(
        gathered,
        lax.all_gather(up_weight, "sp", axis=0, tiled=True),
        preferred_element_type=jnp.float32,
    )
    hidden = (jax.nn.silu(gate_part) * up_part).astype(jnp.bfloat16)
    partial_terms = jnp.dot(
        hidden,
        lax.all_gather(down_weight, "sp", axis=1, tiled=True),
        preferred_element_type=jnp.float32,
    )
    lowered = lax.psum_scatter(
        partial_terms.astype(jnp.bfloat16), "tp", scatter_dimension=0, tiled=True
    ).astype(jnp.float32)
    lowered = lax.optimization_barrier(lowered.astype(jnp.bfloat16)).astype(jnp.float32)
    result = layer_norm(ALPHA * normed.astype(jnp.float32) + lowered, ffn_gain, ffn_bias)
    return result.astype(jnp.bfloat16)


def solution(mesh):
    placed = (
        P("sp", "tp"),
        P("sp", "tp"),
        P("sp", "tp"),
        P("sp", "tp"),
        P("sp", None),
        P("tp", None),
        P(),
        P(),
        P("sp", "tp"),
        P("sp", "tp"),
        P("tp", "sp"),
        P(),
        P(),
    )
    return jax.shard_map(
        body, mesh=mesh, in_specs=placed, out_specs=P(("sp", "tp"), None), check_vma=False
    )
```

profile of v0, /device:TPU:0, one launch (start us, length us, event | category | flops | bytes accessed | tf_op | source)
XLA Modules:
  0.0 859.3 jit_solution(4486789846693739934)
XLA Ops:
  6.5 0.0 copy-start
  6.5 0.0 all-gather.7.cloned.1.call-start
  6.5 0.7 all-gather.7.cloned.1.call-update
  7.3 0.0 all-gather.9.cloned.1.call-start
  7.3 0.7 all-gather.9.cloned.1.call-update
  8.0 0.0 reduce-scatter.3.cloned.1.call-start
  8.1 1.4 copy.18
  9.5 0.0 copy-done.6
  9.5 35.9 %all_gather.22 = f32[6144,8]{0,1:T(8,128)} all-gather(f32[768,8]{0,1:T(8,128)S(1)} %copy-done.6), channel_id=1, replica_groups=mesh['sp'=8,'tp'=4] {'sp'}, dimensions={0}, use_global_device_ids=true | all-gather | bytes 221184 | tf_op jit(solution)/shard_map/all_gather | solution.py:26
  45.4 66.8 %all-gather.7.cloned.1.call-done = bf16[6144,512]{1,0:T(8,128)(2,1)} async-done(((bf16[768,512]{1,0:T(8,128)(2,1)}), bf16[6144,512]{1,0:T(8,128)(2,1)}) %all-gather.7.cloned.1.call-update) | async-done | bytes 6291472 | tf_op jit(solution)/shard_map/all_gather | solution.py:33
  112.2 16.3 %reshape.82 = bf16[8,768,8,64]{3,2,1,0:T(8,128)(2,1)} reshape(bf16[6144,512]{1,0:T(8,128)(2,1)} %all-gather.7.cloned.1.call-done) | data formatting | bytes 12582912 | tf_op jit(solution)/shard_map/reshape | solution.py:46
  128.4 13.3 %copy.20 = bf16[8,768,8,64]{1,3,2,0:T(8,128)(2,1)} copy(bf16[8,768,8,64]{3,2,1,0:T(8,128)(2,1)} %reshape.82) | data formatting | bytes 12582912
  141.7 69.5 %all-gather.9.cloned.1.call-done = bf16[6144,512]{1,0:T(8,128)(2,1)} async-done(((bf16[768,512]{1,0:T(8,128)(2,1)}), bf16[6144,512]{1,0:T(8,128)(2,1)}) %all-gather.9.cloned.1.call-update) | async-done | bytes 6291472 | tf_op jit(solution)/shard_map/all_gather | solution.py:34
  211.2 16.2 %reshape.83 = bf16[8,768,8,64]{3,2,1,0:T(8,128)(2,1)} reshape(bf16[6144,512]{1,0:T(8,128)(2,1)} %all-gather.9.cloned.1.call-done) | data formatting | bytes 12582912 | tf_op jit(solution)/shard_map/reshape | solution.py:47
  227.5 13.2 %copy.21 = bf16[8,768,8,64]{1,3,2,0:T(8,128)(2,1)} copy(bf16[8,768,8,64]{3,2,1,0:T(8,128)(2,1)} %reshape.83) | data formatting | bytes 12582912
  240.6 1.3 broadcast_in_dim.52
  242.0 34.5 %while.15 = (s32[]{:T(128)}, f32[8,768]{1,0:T(8,128)S(1)}, f32[8,768]{1,0:T(8,128)S(1)}, f32[768,8,64]{0,2,1:T(8,128)}, s32[8]{0:T(128)S(1)}, /*index=5*/s32[]{:...) while((s32[]{:T(128)}, f32[8,768]{1,0:T(8,128)S(1)}, ...), condition=%wide.region_5.6_spmd.clone, body=%wide.region_0.5_spmd.clone.sunk | while | flops 1299009024 | bytes 77679992 | solution.py:83
  242.0 0.6 dynamic_slice.50
  243.2 23.8 %conditional.3 = ((f32[8,768]{1,0:T(8,128)S(1)}, f32[8,768]{1,0:T(8,128)S(1)}, f32[768,8,64]{0,2,1:T(8,128)})) conditional(s32[]{:T(128)} %convert_element_type.96, (f32[8,768]{1,0:T(8,128)S(1)}, f32[8,768]{1,0:T(8,128)S(1)}, f32[768,8,64]{0,2,1:T(8,128)}) %tuple.40, (s32[]{:T(128)}, s32[]{:T(128)}, bf16[8,768,8,64]{1,3,2,0:T(8,128)(2,1)}, s32[]{:T(128)}, ...), branch_computations={%region_1.1_spmd, %region_2.4_spmd} | conditional | flops 1299009024 | bytes 77676648 | solution.py:81
  243.2 0.6 iota_add_fusion
  243.9 0.4 broadcast_compare_fusion
  244.3 0.7 dynamic-slice_bitcast_fusion
  245.0 6.6 fusion.4
  251.6 0.0 copy-done.4
  251.7 8.0 bitcast_add_fusion
  259.7 0.0 copy-start.5
  259.7 7.3 fusion.3
  267.0 0.0 copy-done.5
  267.1 0.6 dynamic_slice.50
  268.4 0.6 dynamic_slice.50
  269.7 0.6 dynamic_slice.50
  271.0 0.6 dynamic_slice.50
  272.3 0.6 dynamic_slice.50
  273.6 0.6 dynamic_slice.50
  274.9 0.6 dynamic_slice.50
  276.4 1.5 divide_convert_fusion
  278.0 0.0 copy-done
  278.0 3.5 convolution_convert_fusion
  281.5 0.0 reduce-scatter.3.cloned.1.call-update
  281.6 0.0 all-gather.13.cloned.1.call-start
  281.6 0.5 all-gather.13.cloned.1.call-update
  282.1 0.0 all-gather.11.cloned.1.call-start
  282.2 202.4 %reduce-scatter.3.cloned.1.call-done = bf16[192,2048]{1,0:T(8,128)(2,1)} async-done(((bf16[768,2048]{1,0:T(8,128)(2,1)}), bf16[192,2048]{1,0:T(8,128)(2,1)}) %reduce-scatter.3.cloned.1.call-update) | async-done | bytes 786448 | tf_op jit(solution)/shard_map/reduce_scatter | solution.py:109
  484.6 1.8 fusion.21
  486.4 1.8 multiply_reduce_fusion.1
  488.2 2.5 add_convert_fusion.1
  490.7 0.0 all-gather.11.cloned.1.call-update
  490.8 0.0 all-gather.15.cloned.1.call-start
  490.8 0.5 all-gather.15.cloned.1.call-update
  491.3 0.0 all-gather.17.cloned.1.call-start
  491.4 0.7 all-gather.17.cloned.1.call-update
  492.1 0.0 reduce-scatter.5.cloned.1.call-start
  492.1 86.8 %all-gather.13.cloned.1.call-done = bf16[2048,1408]{1,0:T(8,128)(2,1)} async-done(((bf16[256,1408]{1,0:T(8,128)(2,1)}), bf16[2048,1408]{1,0:T(8,128)(2,1)}) %all-gather.13.cloned.1.call-update) | async-done | bytes 5767184 | tf_op jit(solution)/shard_map/all_gather | solution.py:123
  579.0 28.1 %all-gather.11.cloned.1.call-done = bf16[768,2048]{1,0:T(8,128)(2,1)} async-done(((bf16[192,2048]{1,0:T(8,128)(2,1)}), bf16[768,2048]{1,0:T(8,128)(2,1)}) %all-gather.11.cloned.1.call-update) | async-done | bytes 3145744 | tf_op jit(solution)/shard_map/all_gather | solution.py:120
  607.1 9.7 %fusion.24 = f32[768,1408]{1,0:T(8,128)} fusion(bf16[768,2048]{1,0:T(8,128)(2,1)} %all-gather.11.cloned.1.call-done, bf16[2048,1408]{1,0:T(8,128)(2,1)} %all-gather.13.cloned.1.call-done), kind=kOutput, calls=%fused_computation.44 | convolution fusion | flops 4429185024 | bytes 13238272 | tf_op jit(solution)/shard_map/dot_general | solution.py:121
  616.8 84.7 %all-gather.15.cloned.1.call-done = bf16[2048,1408]{1,0:T(8,128)(2,1)} async-done(((bf16[256,1408]{1,0:T(8,128)(2,1)}), bf16[2048,1408]{1,0:T(8,128)(2,1)}) %all-gather.15.cloned.1.call-update) | async-done | bytes 5767184 | tf_op jit(solution)/shard_map/all_gather | solution.py:128
  701.5 93.4 %all-gather.17.cloned.1.call-done = bf16[1408,2048]{1,0:T(8,128)(2,1)} async-done(((bf16[1408,256]{1,0:T(8,128)(2,1)}), bf16[1408,2048]{1,0:T(8,128)(2,1)}) %all-gather.17.cloned.1.call-update) | async-done | bytes 5767184 | tf_op jit(solution)/shard_map/all_gather | solution.py:134
  794.9 16.8 %convolution_convert_fusion.1 = bf16[768,2048]{1,0:T(8,128)(2,1)} fusion(bf16[1408,2048]{1,0:T(8,128)(2,1)} %all-gather.17.cloned.1.call-done, f32[768,1408]{1,0:T(8,128)} %fusion.24, bf16[768,2048]{1,0:T(8,128)(2,1)} %all-gather.11.cloned.1.call-done, bf16[2048,1408]{1,0:T(8,128)(2,1)} %all-gather.15.cloned.1.call-done), kind=kOutput, calls=%fused_computation.28 | convolution fusion | flops 8866430976 | bytes 22151168 | tf_op jit(solution)/shard_map/dot_general | solution.py:132
  811.7 0.0 reduce-scatter.5.cloned.1.call-update
  811.7 36.2 %reduce-scatter.5.cloned.1.call-done = bf16[192,2048]{1,0:T(8,128)(2,1)} async-done(((bf16[768,2048]{1,0:T(8,128)(2,1)}), bf16[192,2048]{1,0:T(8,128)(2,1)}) %reduce-scatter.5.cloned.1.call-update) | async-done | bytes 786448 | tf_op jit(solution)/shard_map/reduce_scatter | solution.py:137
  847.9 1.5 fusion.22
  849.5 1.6 multiply_reduce_fusion
  851.0 0.0 copy-done.9
  851.1 1.3 add_convert_fusion
  (40 shorter events, 0.2 us)
Async XLA Ops:
  6.5 271.4 %copy-start = (bf16[512,2048]{1,0:T(8,128)(2,1)S(1)}, bf16[512,2048]{1,0:T(8,128)(2,1)}, u32[]{:S(2)}) copy-start(bf16[512,2048]{1,0:T(8,128)(2,1)} %param.22) | copy-start | bytes 6291460
  6.5 2.9 copy-start.6
  6.5 105.6 %all-gather.7.cloned.1.call-start = ((), (), s32[]{:S(2)}) async-start(), calls=%async_computation.2 | async-start | bytes 7077888 | tf_op jit(solution)/shard_map/all_gather | solution.py:33
  7.3 204.0 %all-gather.9.cloned.1.call-start = ((), (), s32[]{:S(2)}) async-start(), calls=%async_computation.3 | async-start | bytes 7077888 | tf_op jit(solution)/shard_map/all_gather | solution.py:34
  8.0 476.6 %reduce-scatter.3.cloned.1.call-start = ((), (), s32[]{:S(2)}) async-start(), calls=%async_computation.4 | async-start | bytes 3932160 | tf_op jit(solution)/shard_map/reduce_scatter | solution.py:109
  245.0 6.6 copy-start.4
  259.7 7.4 copy-start.5
  281.5 206.7 %copy-start.7 = (f32[2048]{0:T(1024)S(1)}, f32[2048]{0:T(1024)}, u32[]{:S(2)}) copy-start(f32[2048]{0:T(1024)} %param.24) | copy-start | bytes 24580
  281.5 206.7 %copy-start.8 = (f32[2048]{0:T(1024)S(1)}, f32[2048]{0:T(1024)}, u32[]{:S(2)}) copy-start(f32[2048]{0:T(1024)} %param.23) | copy-start | bytes 24580
  281.6 297.4 %all-gather.13.cloned.1.call-start = ((), (), s32[]{:S(2)}) async-start(), calls=%async_computation.6 | async-start | bytes 6488064 | tf_op jit(solution)/shard_map/all_gather | solution.py:123
  282.1 325.0 %all-gather.11.cloned.1.call-start = ((), (), s32[]{:S(2)}) async-start(), calls=%async_computation.5 | async-start | bytes 3932160 | tf_op jit(solution)/shard_map/all_gather | solution.py:120
  484.6 3.6 copy-start.2
  490.8 210.7 %all-gather.15.cloned.1.call-start = ((), (), s32[]{:S(2)}) async-start(), calls=%async_computation.7 | async-start | bytes 6488064 | tf_op jit(solution)/shard_map/all_gather | solution.py:128
  491.3 303.5 %all-gather.17.cloned.1.call-start = ((), (), s32[]{:S(2)}) async-start(), calls=%async_computation.8 | async-start | bytes 6488064 | tf_op jit(solution)/shard_map/all_gather | solution.py:134
  492.1 355.8 %reduce-scatter.5.cloned.1.call-start = ((), (), s32[]{:S(2)}) async-start(), calls=%async_computation.9 | async-start | bytes 3932160 | tf_op jit(solution)/shard_map/reduce_scatter | solution.py:137
  811.6 36.3 %copy-start.1 = (bf16[192,2048]{1,0:T(8,128)(2,1)S(1)}, bf16[192,2048]{1,0:T(8,128)(2,1)}, u32[]{:S(2)}) copy-start(bf16[192,2048]{1,0:T(8,128)(2,1)} %add_convert_fusion.1) | copy-start | bytes 2359300
  811.6 39.4 %copy-start.9 = (f32[2048]{0:T(1024)S(1)}, f32[2048]{0:T(1024)}, u32[]{:S(2)}) copy-start(f32[2048]{0:T(1024)} %param.29) | copy-start | bytes 24580
  811.6 39.4 %copy-start.10 = (f32[2048]{0:T(1024)S(1)}, f32[2048]{0:T(1024)}, u32[]{:S(2)}) copy-start(f32[2048]{0:T(1024)} %param.28) | copy-start | bytes 24580
  847.9 3.2 copy-start.3
Sparse Core Ops, SparseCore 0:
  9.5 102.5 all-gather.6
  114.3 96.8 all-gather.8
  281.7 202.8 reduce-scatter.2
  486.6 92.2 all-gather.12
  580.4 26.6 all-gather.10
  609.1 92.3 all-gather.14
  703.5 91.2 all-gather.16
  811.8 36.0 reduce-scatter.4
where the time goes:
time: 862 us; the launch traced here: 859 us
  waiting for transfers between devices  671 us (78%)
  local copies, waits for them, and re-layouts  67.6 us (8%)
  matrix products  44.6 us (5%)
  blocking collectives  35.9 us (4%)
  other arithmetic  20.5 us (2%)
  between operations  13.6 us (2%)
    reduce_scatter x1, waiting for transfers between devices, body(): lax.psum_scatter(jnp.dot(attended, out_weight, preferred_element_type=jnp...  202 us
    all_gather x1, waiting for transfers between devices, body(): lax.all_gather(down_weight, 'sp', axis=1, tiled=True)  93.4 us
    all_gather x1, waiting for transfers between devices, body(): lax.all_gather(gate_weight, 'sp', axis=0, tiled=True)  86.8 us
    all_gather x1, waiting for transfers between devices, body(): lax.all_gather(up_weight, 'sp', axis=0, tiled=True)  84.7 us
    all_gather x1, waiting for transfers between devices, attend(): value_piece = lax.all_gather(value_rows, 'sp', axis=0, tiled=True)  69.5 us
    all_gather x1, waiting for transfers between devices, attend(): key_piece = lax.all_gather(key_rows, 'sp', axis=0, tiled=True)  66.8 us
    reduce_scatter x1, waiting for transfers between devices, body(): lax.psum_scatter(partial_terms.astype(jnp.bfloat16), 'tp', scatter_dimens...  36.2 us
    all_gather x1, blocking collectives, attend(): gates_all = lax.all_gather(log_forget, 'sp', axis=0, tiled=True)  35.9 us
  transfers between devices with their start and end apart: 8, of which 8 were waited for; matrix products, arithmetic and copies ran while one was open for 5% of the time, Pallas kernels for 0%

commit v1 on v0

--- a/solution.py
+++ b/solution.py
@@ -31,7 +31,12 @@
     )
     running = initial
     key_piece = lax.all_gather(key_rows, "sp", axis=0, tiled=True)
-    value_piece = lax.all_gather(value_rows, "sp", axis=0, tiled=True)
+    ring = [value_rows]
+    for hop in range(7):
+        ring.append(lax.ppermute(ring[-1], "sp", [(dev, (dev + 1) % 8) for dev in range(8)]))
+    value_piece = jnp.roll(
+        jnp.concatenate(ring[::-1], axis=0), (lax.axis_index("sp") + 1) * ring[0].shape[0], axis=0
+    )
     piece_len = key_piece.shape[0]
     shards = piece_len // length
     group_size = max(

time: 862 us -> 940 us (1.090)
  waiting for transfers between devices: 671 us -> 718 us
  local copies, waits for them, and re-layouts: 67.6 us -> 84.5 us
    ppermute x0 -> x7, waiting for transfers between devices: none -> 186 us  [attend(): lax.ppermute(ring[-1], 'sp', [(dev, (dev + 1) % 8) for dev in range(8)])]
    all_gather x1 -> x0, waiting for transfers between devices: 69.5 us -> none  [attend(): value_piece = lax.all_gather(value_rows, 'sp', axis=0, tiled=True)]
    all_gather x1, waiting for transfers between devices: 66.8 us -> 0.01 us  [attend(): key_piece = lax.all_gather(key_rows, 'sp', axis=0, tiled=True)]
    unnamed x21 -> x56, local copies, waits for them, and re-layouts: 27.9 us -> 40.9 us
  transfers between devices with their start and end apart: 8 -> 14, of which waited for: 8 -> 12; matrix products, arithmetic and copies ran while one was open for 5% -> 6% of each run, Pallas kernels for 0% -> 0%
where the time goes in v1:
time: 940 us; the launch traced here: 937 us
  waiting for transfers between devices  718 us (76%)
  local copies, waits for them, and re-layouts  84.5 us (9%)
  matrix products  44.6 us (5%)
  blocking collectives  44.3 us (5%)
  other arithmetic  21.7 us (2%)
  between operations  13.8 us (1%)
    reduce_scatter x1, waiting for transfers between devices, body(): lax.psum_scatter(jnp.dot(attended, out_weight, preferred_element_type=jnp...  200 us
    ppermute x7, waiting for transfers between devices, attend(): lax.ppermute(ring[-1], 'sp', [(dev, (dev + 1) % 8) for dev in range(8)])  186 us
    all_gather x1, waiting for transfers between devices, body(): lax.all_gather(down_weight, 'sp', axis=1, tiled=True)  93.2 us
    all_gather x1, waiting for transfers between devices, body(): lax.all_gather(gate_weight, 'sp', axis=0, tiled=True)  87 us
    all_gather x1, waiting for transfers between devices, body(): lax.all_gather(up_weight, 'sp', axis=0, tiled=True)  84.7 us
    all_gather x1, blocking collectives, attend(): gates_all = lax.all_gather(log_forget, 'sp', axis=0, tiled=True)  44.3 us
    unnamed x56, local copies, waits for them, and re-layouts  40.9 us
    reduce_scatter x1, waiting for transfers between devices, body(): lax.psum_scatter(partial_terms.astype(jnp.bfloat16), 'tp', scatter_dimens...  36.2 us
  transfers between devices with their start and end apart: 14, of which 12 were waited for; matrix products, arithmetic and copies ran while one was open for 6% of the time, Pallas kernels for 0%

profile of v1, /device:TPU:0, one launch (start us, length us, event | category | flops | bytes accessed | tf_op | source)
XLA Modules:
  0.0 936.9 jit_solution(813044454784271184)
XLA Ops:
  6.5 0.7 all-gather.6.cloned.1.call-update
  7.3 3.0 collective-permute-start
  10.4 26.5 %collective-permute-done = bf16[768,512]{1,0:T(8,128)(2,1)S(1)} collective-permute-done((bf16[768,512]{1,0:T(8,128)(2,1)}, bf16[768,512]{1,0:T(8,128)(2,1)S(1)}, u32[]{:S(2)}, u32[]{:S(2)}) %collective-permute-start) | collective-permute-done | bytes 786464 | tf_op jit(solution)/shard_map/ppermute | solution.py:36
  36.9 0.9 copy-done.5
  37.8 0.5 collective-permute-start.1
  38.3 35.1 %collective-permute-done.1 = bf16[768,512]{1,0:T(8,128)(2,1)S(1)} collective-permute-done((bf16[768,512]{1,0:T(8,128)(2,1)S(1)}, bf16[768,512]{1,0:T(8,128)(2,1)S(1)}, u32[]{:S(2)}, u32[]{:S(2)}) %collective-permute-start.1) | collective-permute-done | bytes 786464 | tf_op jit(solution)/shard_map/ppermute | solution.py:36
  73.4 0.9 copy-done.7
  74.3 38.9 %collective-permute-done.2 = bf16[768,512]{1,0:T(8,128)(2,1)S(1)} collective-permute-done((bf16[768,512]{1,0:T(8,128)(2,1)S(1)}, bf16[768,512]{1,0:T(8,128)(2,1)S(1)}, u32[]{:S(2)}, u32[]{:S(2)}) %collective-permute-start.2) | collective-permute-done | bytes 786464 | tf_op jit(solution)/shard_map/ppermute | solution.py:36
  113.2 0.9 copy-done.9
  114.1 38.7 %collective-permute-done.3 = bf16[768,512]{1,0:T(8,128)(2,1)S(1)} collective-permute-done((bf16[768,512]{1,0:T(8,128)(2,1)S(1)}, bf16[768,512]{1,0:T(8,128)(2,1)S(1)}, u32[]{:S(2)}, u32[]{:S(2)}) %collective-permute-start.3) | collective-permute-done | bytes 786464 | tf_op jit(solution)/shard_map/ppermute | solution.py:36
  152.8 0.9 copy-done.11
  153.7 26.2 %collective-permute-done.4 = bf16[768,512]{1,0:T(8,128)(2,1)S(1)} collective-permute-done((bf16[768,512]{1,0:T(8,128)(2,1)S(1)}, bf16[768,512]{1,0:T(8,128)(2,1)S(1)}, u32[]{:S(2)}, u32[]{:S(2)}) %collective-permute-start.4) | collective-permute-done | bytes 786464 | tf_op jit(solution)/shard_map/ppermute | solution.py:36
  179.9 0.9 copy-done.13
  180.8 20.9 %collective-permute-done.5 = bf16[768,512]{1,0:T(8,128)(2,1)} collective-permute-done((bf16[768,512]{1,0:T(8,128)(2,1)S(1)}, bf16[768,512]{1,0:T(8,128)(2,1)}, u32[]{:S(2)}, u32[]{:S(2)}) %collective-permute-start.5) | collective-permute-done | bytes 786464 | tf_op jit(solution)/shard_map/ppermute | solution.py:36
  201.7 2.3 copy.18
  204.0 44.3 %all_gather.19 = f32[6144,8]{0,1:T(8,128)} all-gather(f32[768,8]{0,1:T(8,128)} %param.20), channel_id=1, replica_groups=mesh['sp'=8,'tp'=4] {'sp'}, dimensions={0}, use_global_device_ids=true | all-gather | bytes 221184 | tf_op jit(solution)/shard_map/all_gather | solution.py:26
  248.3 1.2 constant_dynamic-update-slice_fusion.15
  249.5 1.2 constant_dynamic-update-slice_fusion.14
  250.7 1.2 constant_dynamic-update-slice_fusion.13
  251.8 1.3 constant_dynamic-update-slice_fusion.12
  253.1 0.1 constant_dynamic-update-slice_fusion.11
  253.4 1.2 constant_dynamic-update-slice_fusion.7
  254.6 1.2 constant_dynamic-update-slice_fusion.6
  256.2 4.2 constant_dynamic-slice_fusion
  260.4 16.2 %reshape.83 = bf16[8,768,8,64]{3,2,1,0:T(8,128)(2,1)} reshape(bf16[6144,512]{1,0:T(8,128)(2,1)} %constant_dynamic-slice_fusion) | data formatting | bytes 12582912 | tf_op jit(solution)/shard_map/reshape | solution.py:52
  276.6 13.1 %copy.21 = bf16[8,768,8,64]{1,3,2,0:T(8,128)(2,1)} copy(bf16[8,768,8,64]{3,2,1,0:T(8,128)(2,1)} %reshape.83) | data formatting | bytes 12582912
  289.8 16.2 %reshape.82 = bf16[8,768,8,64]{3,2,1,0:T(8,128)(2,1)} reshape(bf16[6144,512]{1,0:T(8,128)(2,1)} %all-gather.6.cloned.1.call-done) | data formatting | bytes 12582912 | tf_op jit(solution)/shard_map/reshape | solution.py:51
  306.0 13.3 %copy.20 = bf16[8,768,8,64]{1,3,2,0:T(8,128)(2,1)} copy(bf16[8,768,8,64]{3,2,1,0:T(8,128)(2,1)} %reshape.82) | data formatting | bytes 12582912
  319.2 1.3 broadcast_in_dim.52
  320.6 34.5 %while.15 = (s32[]{:T(128)}, f32[8,768]{1,0:T(8,128)S(1)}, f32[8,768]{1,0:T(8,128)S(1)}, f32[768,8,64]{0,2,1:T(8,128)}, s32[8]{0:T(128)S(1)}, /*index=5*/s32[]{:...) while((s32[]{:T(128)}, f32[8,768]{1,0:T(8,128)S(1)}, ...), condition=%wide.region_5.6_spmd.clone, body=%wide.region_0.5_spmd.clone.sunk | while | flops 1299009024 | bytes 77679992 | solution.py:88
  320.8 0.6 dynamic_slice.56
  322.0 23.9 %conditional.3 = ((f32[8,768]{1,0:T(8,128)S(1)}, f32[8,768]{1,0:T(8,128)S(1)}, f32[768,8,64]{0,2,1:T(8,128)})) conditional(s32[]{:T(128)} %convert_element_type.96, (f32[8,768]{1,0:T(8,128)S(1)}, f32[8,768]{1,0:T(8,128)S(1)}, f32[768,8,64]{0,2,1:T(8,128)}) %tuple.40, (s32[]{:T(128)}, s32[]{:T(128)}, bf16[8,768,8,64]{1,3,2,0:T(8,128)(2,1)}, s32[]{:T(128)}, ...), branch_computations={%region_1.1_spmd, %region_2.4_spmd} | conditional | flops 1299009024 | bytes 77676648 | solution.py:86
  322.0 0.7 iota_add_fusion
  322.7 0.4 broadcast_compare_fusion
  323.1 0.7 dynamic-slice_bitcast_fusion
  323.9 6.6 fusion.4
  330.5 8.0 bitcast_add_fusion
  338.5 7.3 fusion.3
  345.9 0.6 dynamic_slice.56
  347.2 0.6 dynamic_slice.56
  348.5 0.6 dynamic_slice.56
  349.8 0.6 dynamic_slice.56
  351.0 0.6 dynamic_slice.56
  352.3 0.6 dynamic_slice.56
  353.6 0.6 dynamic_slice.56
  355.1 1.5 divide_convert_fusion
  356.7 3.5 convolution_convert_fusion
  360.3 0.7 all-gather.10.cloned.1.call-update
  361.0 200.2 %reduce-scatter.3.cloned.1.call-done = bf16[192,2048]{1,0:T(8,128)(2,1)} async-done(((bf16[768,2048]{1,0:T(8,128)(2,1)}), bf16[192,2048]{1,0:T(8,128)(2,1)}) %reduce-scatter.3.cloned.1.call-update) | async-done | bytes 786448 | tf_op jit(solution)/shard_map/reduce_scatter | solution.py:114
  561.2 1.7 fusion.21
  562.9 1.8 multiply_reduce_fusion.1
  564.8 2.7 add_convert_fusion.1
  567.6 0.5 all-gather.12.cloned.1.call-update
  568.2 0.5 all-gather.14.cloned.1.call-update
  568.7 87.0 %all-gather.10.cloned.1.call-done = bf16[2048,1408]{1,0:T(8,128)(2,1)} async-done(((bf16[256,1408]{1,0:T(8,128)(2,1)}), bf16[2048,1408]{1,0:T(8,128)(2,1)}) %all-gather.10.cloned.1.call-update) | async-done | bytes 5767184 | tf_op jit(solution)/shard_map/all_gather | solution.py:128
  655.8 28.1 %all-gather.8.cloned.1.call-done = bf16[768,2048]{1,0:T(8,128)(2,1)} async-done(((bf16[192,2048]{1,0:T(8,128)(2,1)}), bf16[768,2048]{1,0:T(8,128)(2,1)}) %all-gather.8.cloned.1.call-update) | async-done | bytes 3145744 | tf_op jit(solution)/shard_map/all_gather | solution.py:125
  683.9 9.7 %fusion.24 = f32[768,1408]{1,0:T(8,128)} fusion(bf16[768,2048]{1,0:T(8,128)(2,1)} %all-gather.8.cloned.1.call-done, bf16[2048,1408]{1,0:T(8,128)(2,1)} %all-gather.10.cloned.1.call-done), kind=kOutput, calls=%fused_computation.61 | convolution fusion | flops 4429185024 | bytes 13238272 | tf_op jit(solution)/shard_map/dot_general | solution.py:126
  693.6 84.7 %all-gather.12.cloned.1.call-done = bf16[2048,1408]{1,0:T(8,128)(2,1)} async-done(((bf16[256,1408]{1,0:T(8,128)(2,1)}), bf16[2048,1408]{1,0:T(8,128)(2,1)}) %all-gather.12.cloned.1.call-update) | async-done | bytes 5767184 | tf_op jit(solution)/shard_map/all_gather | solution.py:133
  778.3 93.2 %all-gather.14.cloned.1.call-done = bf16[1408,2048]{1,0:T(8,128)(2,1)} async-done(((bf16[1408,256]{1,0:T(8,128)(2,1)}), bf16[1408,2048]{1,0:T(8,128)(2,1)}) %all-gather.14.cloned.1.call-update) | async-done | bytes 5767184 | tf_op jit(solution)/shard_map/all_gather | solution.py:139
  871.5 16.8 %convolution_convert_fusion.1 = bf16[768,2048]{1,0:T(8,128)(2,1)} fusion(bf16[1408,2048]{1,0:T(8,128)(2,1)} %all-gather.14.cloned.1.call-done, f32[768,1408]{1,0:T(8,128)} %fusion.24, bf16[768,2048]{1,0:T(8,128)(2,1)} %all-gather.8.cloned.1.call-done, bf16[2048,1408]{1,0:T(8,128)(2,1)} %all-gather.12.cloned.1.call-done), kind=kOutput, calls=%fused_computation.28 | convolution fusion | flops 8866430976 | bytes 22151168 | tf_op jit(solution)/shard_map/dot_general | solution.py:137
  888.3 36.2 %reduce-scatter.5.cloned.1.call-done = bf16[192,2048]{1,0:T(8,128)(2,1)} async-done(((bf16[768,2048]{1,0:T(8,128)(2,1)}), bf16[192,2048]{1,0:T(8,128)(2,1)}) %reduce-scatter.5.cloned.1.call-update) | async-done | bytes 786448 | tf_op jit(solution)/shard_map/reduce_scatter | solution.py:142
  924.5 1.5 fusion.22
  926.0 1.6 multiply_reduce_fusion
  927.6 2.5 add_convert_fusion
  (88 shorter events, 1.0 us)
Async XLA Ops:
  6.5 350.1 %copy-start = (bf16[512,2048]{1,0:T(8,128)(2,1)S(1)}, bf16[512,2048]{1,0:T(8,128)(2,1)}, u32[]{:S(2)}) copy-start(bf16[512,2048]{1,0:T(8,128)(2,1)} %param.22) | copy-start | bytes 6291460
  6.5 283.2 %all-gather.6.cloned.1.call-start = ((), (), s32[]{:S(2)}) async-start(), calls=%async_computation.2 | async-start | bytes 7077888 | tf_op jit(solution)/shard_map/all_gather | solution.py:33
  7.3 554.0 %reduce-scatter.3.cloned.1.call-start = ((), (), s32[]{:S(2)}) async-start(), calls=%async_computation.3 | async-start | bytes 3932160 | tf_op jit(solution)/shard_map/reduce_scatter | solution.py:114
  7.3 29.6 %collective-permute-start = (bf16[768,512]{1,0:T(8,128)(2,1)}, bf16[768,512]{1,0:T(8,128)(2,1)S(1)}, u32[]{:S(2)}, u32[]{:S(2)}) collective-permute-start(bf16[768,512]{1,0:T(8,128)(2,1)} %param.19), channel_id=1, source_target_pairs={{0,4},{4,8},{8,12},{12,16},{16,20},{20,24},{24,28},{28,0},{1,5},{5... | collective-permute-start | bytes 2359304 | tf_op jit(solution)/shard_map/ppermute | solution.py:36
  36.9 0.9 copy-start.5
  37.8 35.6 %collective-permute-start.1 = (bf16[768,512]{1,0:T(8,128)(2,1)S(1)}, bf16[768,512]{1,0:T(8,128)(2,1)S(1)}, u32[]{:S(2)}, u32[]{:S(2)}) collective-permute-start(bf16[768,512]{1,0:T(8,128)(2,1)S(1)} %collective-permute-done), channel_id=1, source_target_pairs={{0,4},{4,8},{8,12},{12,16},{16,20},{20,24},{24,28},{28,0},{1,5},{5... | collective-permute-start | bytes 2359304 | tf_op jit(solution)/shard_map/ppermute | solution.py:36
  73.4 0.9 copy-start.7
  74.3 38.9 %collective-permute-start.2 = (bf16[768,512]{1,0:T(8,128)(2,1)S(1)}, bf16[768,512]{1,0:T(8,128)(2,1)S(1)}, u32[]{:S(2)}, u32[]{:S(2)}) collective-permute-start(bf16[768,512]{1,0:T(8,128)(2,1)S(1)} %collective-permute-done.1), channel_id=1, source_target_pairs={{0,4},{4,8},{8,12},{12,16},{16,20},{20,24},{24,28},{28,0},{1,5},{5... | collective-permute-start | bytes 2359304 | tf_op jit(solution)/shard_map/ppermute | solution.py:36
  113.2 0.9 copy-start.9
  114.1 38.7 %collective-permute-start.3 = (bf16[768,512]{1,0:T(8,128)(2,1)S(1)}, bf16[768,512]{1,0:T(8,128)(2,1)S(1)}, u32[]{:S(2)}, u32[]{:S(2)}) collective-permute-start(bf16[768,512]{1,0:T(8,128)(2,1)S(1)} %collective-permute-done.2), channel_id=1, source_target_pairs={{0,4},{4,8},{8,12},{12,16},{16,20},{20,24},{24,28},{28,0},{1,5},{5... | collective-permute-start | bytes 2359304 | tf_op jit(solution)/shard_map/ppermute | solution.py:36
  152.8 0.9 copy-start.11
  153.7 26.2 %collective-permute-start.4 = (bf16[768,512]{1,0:T(8,128)(2,1)S(1)}, bf16[768,512]{1,0:T(8,128)(2,1)S(1)}, u32[]{:S(2)}, u32[]{:S(2)}) collective-permute-start(bf16[768,512]{1,0:T(8,128)(2,1)S(1)} %collective-permute-done.3), channel_id=1, source_target_pairs={{0,4},{4,8},{8,12},{12,16},{16,20},{20,24},{24,28},{28,0},{1,5},{5... | collective-permute-start | bytes 2359304 | tf_op jit(solution)/shard_map/ppermute | solution.py:36
  179.9 0.9 copy-start.13
  180.8 20.9 %collective-permute-start.5 = (bf16[768,512]{1,0:T(8,128)(2,1)S(1)}, bf16[768,512]{1,0:T(8,128)(2,1)}, u32[]{:S(2)}, u32[]{:S(2)}) collective-permute-start(bf16[768,512]{1,0:T(8,128)(2,1)S(1)} %collective-permute-done.4), channel_id=1, source_target_pairs={{0,4},{4,8},{8,12},{12,16},{16,20},{20,24},{24,28},{28,0},{1,5},{5... | collective-permute-start | bytes 2359304 | tf_op jit(solution)/shard_map/ppermute | solution.py:36
  201.7 46.6 %collective-permute-start.6 = (bf16[768,512]{1,0:T(8,128)(2,1)}, bf16[768,512]{1,0:T(8,128)(2,1)}, u32[]{:S(2)}, u32[]{:S(2)}) collective-permute-start(bf16[768,512]{1,0:T(8,128)(2,1)} %collective-permute-done.5), channel_id=1, source_target_pairs={{0,4},{4,8},{8,12},{12,16},{16,20},{20,24},{24,28},{28,0},{1,5},{5... | collective-permute-start | bytes 2359304 | tf_op jit(solution)/shard_map/ppermute | solution.py:36
  204.0 49.4 %copy-start.4 = (bf16[768,512]{1,0:T(8,128)(2,1)S(1)}, bf16[768,512]{1,0:T(8,128)(2,1)}, u32[]{:S(2)}) copy-start(bf16[768,512]{1,0:T(8,128)(2,1)} %param.19) | copy-start | bytes 2359300
  204.0 49.1 %copy-start.10 = (bf16[768,512]{1,0:T(8,128)(2,1)S(1)}, bf16[768,512]{1,0:T(8,128)(2,1)}, u32[]{:S(2)}) copy-start(bf16[768,512]{1,0:T(8,128)(2,1)} %copy-done.9) | copy-start | bytes 2359300
  204.0 49.2 %copy-start.8 = (bf16[768,512]{1,0:T(8,128)(2,1)S(1)}, bf16[768,512]{1,0:T(8,128)(2,1)}, u32[]{:S(2)}) copy-start(bf16[768,512]{1,0:T(8,128)(2,1)} %copy-done.7) | copy-start | bytes 2359300
  204.0 49.3 %copy-start.6 = (bf16[768,512]{1,0:T(8,128)(2,1)S(1)}, bf16[768,512]{1,0:T(8,128)(2,1)}, u32[]{:S(2)}) copy-start(bf16[768,512]{1,0:T(8,128)(2,1)} %copy-done.5) | copy-start | bytes 2359300
  251.8 3.9 copy-start.14
  253.1 2.7 copy-start.12
  306.0 14.6 %copy-start.15 = (f32[768,8]{0,1:T(8,128)S(1)}, f32[768,8]{0,1:T(8,128)}, u32[]{:S(2)}) copy-start(f32[768,8]{0,1:T(8,128)} %param.20) | copy-start | bytes 73732
  306.0 14.6 %copy-start.16 = (bf16[768,512]{0,1:T(8,128)(2,1)S(1)}, bf16[768,512]{0,1:T(8,128)(2,1)}, u32[]{:S(2)}) copy-start(bf16[768,512]{0,1:T(8,128)(2,1)} %copy.18) | copy-start | bytes 2359300
  323.9 6.6 copy-start.2
  338.5 7.4 copy-start.3
  356.6 208.1 %copy-start.17 = (f32[2048]{0:T(1024)S(1)}, f32[2048]{0:T(1024)}, u32[]{:S(2)}) copy-start(f32[2048]{0:T(1024)} %param.24) | copy-start | bytes 24580
  356.7 208.1 %copy-start.18 = (f32[2048]{0:T(1024)S(1)}, f32[2048]{0:T(1024)}, u32[]{:S(2)}) copy-start(f32[2048]{0:T(1024)} %param.23) | copy-start | bytes 24580
  360.2 295.5 %all-gather.10.cloned.1.call-start = ((), (), s32[]{:S(2)}) async-start(), calls=%async_computation.5 | async-start | bytes 6488064 | tf_op jit(solution)/shard_map/all_gather | solution.py:128
  361.0 322.9 %all-gather.8.cloned.1.call-start = ((), (), s32[]{:S(2)}) async-start(), calls=%async_computation.4 | async-start | bytes 3932160 | tf_op jit(solution)/shard_map/all_gather | solution.py:125
  567.5 210.7 %all-gather.12.cloned.1.call-start = ((), (), s32[]{:S(2)}) async-start(), calls=%async_computation.6 | async-start | bytes 6488064 | tf_op jit(solution)/shard_map/all_gather | solution.py:133
  568.1 303.4 %all-gather.14.cloned.1.call-start = ((), (), s32[]{:S(2)}) async-start(), calls=%async_computation.7 | async-start | bytes 6488064 | tf_op jit(solution)/shard_map/all_gather | solution.py:139
  568.7 355.8 %reduce-scatter.5.cloned.1.call-start = ((), (), s32[]{:S(2)}) async-start(), calls=%async_computation.8 | async-start | bytes 3932160 | tf_op jit(solution)/shard_map/reduce_scatter | solution.py:142
  693.6 231.0 %copy-start.1 = (bf16[192,2048]{1,0:T(8,128)(2,1)S(1)}, bf16[192,2048]{1,0:T(8,128)(2,1)}, u32[]{:S(2)}) copy-start(bf16[192,2048]{1,0:T(8,128)(2,1)} %add_convert_fusion.1) | copy-start | bytes 2359300
  888.3 39.3 %copy-start.19 = (f32[2048]{0:T(1024)S(1)}, f32[2048]{0:T(1024)}, u32[]{:S(2)}) copy-start(f32[2048]{0:T(1024)} %param.29) | copy-start | bytes 24580
  888.3 39.3 %copy-start.20 = (f32[2048]{0:T(1024)S(1)}, f32[2048]{0:T(1024)}, u32[]{:S(2)}) copy-start(f32[2048]{0:T(1024)} %param.28) | copy-start | bytes 24580
Sparse Core Ops, SparseCore 0:
  9.5 146.4 all-gather.5
  360.3 200.8 reduce-scatter.2
  563.4 92.2 all-gather.9
  657.2 26.6 all-gather.7
  685.9 92.3 all-gather.11
  780.2 91.2 all-gather.13
  888.4 36.0 reduce-scatter.4
